TPU v7x, 256 devices: a whole 4x4x8 slice. The times are simulated.
256 devices in a mesh: fs: 16 (over y, x), tp: 16 (over z, core).
Axes of the slice: x: 4, y: 4, z: 8, core: 2. Of those that a mesh axis runs over, the one named last changes fastest.
Arguments:
- tokens: bfloat16 [32768, 2048], P(('fs', 'tp')), may hold values from -6 to 6
- norm_gain: float32 [2048], replicated, may hold values from 0.1 to 1.9
- gate_weight: bfloat16 [2048, 5632], P('fs', 'tp'), may hold values from -0.125 to 0.125
- up_weight: bfloat16 [2048, 5632], P('fs', 'tp'), may hold values from -0.125 to 0.125
- down_weight: bfloat16 [5632, 2048], P('tp', 'fs'), may hold values from -0.078125 to 0.078125
Outputs:
- mixed: bfloat16 [32768, 2048], P(('fs', 'tp'))
All inputs are finite; a program needn't handle non-finite values.
Results may differ from a plain program's by a relative error of at most 0.0065.
Values may be sent and summed in bfloat16 or wider, within the bound.
A program may use at most 128 MiB of HBM per device.

v0:
```python
import functools
import math

import jax
import jax.numpy as jnp
from jax import lax
from jax.experimental import pallas as pl
from jax.experimental.pallas import tpu as pltpu

eps_floor = 0.05
MESH = pl.DeviceIdType.MESH
F32 = jnp.float32
BF16 = jnp.bfloat16


def kernel(Y, X, Z, C, cuts, tok, gain, gw, uw, dw, out, nrm, Wg, Wu, Wd, acc_g, acc_u, hid,
           sib_s, sib_r, rs_s, rs_r, part, w_local,
           w_send, w_recv, t_send, t_recv, ts_send, ts_recv, p_send, p_recv, q_send, q_recv):
    F = Y * X
    f = lax.axis_index("fs")
    t = lax.axis_index("tp")
    y, x = f // X, f % X
    z, c = t // C, t % C
    rows, D = tok.shape
    H, K = gw.shape
    N = dw.shape[1] // cuts
    tile = 2 if Z % 2 == 0 else 1

    def fs_at(j, i):
        return lax.rem(y + j, Y) * X + lax.rem(x + i, X)

    def tp_at(zz, cc):
        return zz * C + cc

    sib = lax.rem(c + 1, C)

    barrier = pltpu.get_barrier_semaphore()
    peers = [{"fs": fs_at(0, i)} for i in range(1, X)] + [{"fs": fs_at(j, 0)} for j in range(1, Y)]
    if C > 1:
        peers += [{"tp": tp_at(z, sib)}]

    def greet(peer):
        pl.semaphore_signal(barrier, inc=1, device_id=peer, device_id_type=MESH)

    for peer in peers:
        greet(peer)
    below, above = jnp.maximum(z - 1, 0), jnp.minimum(z + 1, Z - 1)
    pl.when(z > 0)(lambda: greet({"tp": tp_at(below, c)}))
    pl.when(z < Z - 1)(lambda: greet({"tp": tp_at(above, c)}))

    mats = ((gw, Wg), (uw, Wu), (dw, Wd))
    own_copies = [pltpu.make_async_copy(ref, held.at[f], w_local.at[m]) for m, (ref, held) in enumerate(mats)]
    for cp in own_copies:
        cp.start()

    values = tok[...].astype(F32)
    factor = lax.rsqrt(jnp.mean(values * values, axis=-1, keepdims=True) + eps_floor)
    nrm[c, z] = (values * factor * gain[...]).astype(BF16)
    pl.semaphore_wait(barrier, len(peers) + (z > 0).astype(jnp.int32) + (z < Z - 1).astype(jnp.int32))
    for cp in own_copies:
        cp.wait()

    w_copies = []

    def piece(m, h, j, i):
        held = mats[m][1].at[fs_at(j, i)]
        if m == 2 and cuts == 2:
            return held.at[:, pl.ds(h * N, N)]
        n = held.shape[0] // 2
        return held.at[pl.ds(h * n, n)]

    def w_copy(m, h, j, i, dj, di):
        k = len(w_copies)
        slot = ((j - dj) % Y) * X + (i - di) % X
        cp = pltpu.make_async_remote_copy(
            src_ref=piece(m, h, j, i), dst_ref=piece(m, h, j, i),
            send_sem=w_send.at[k], recv_sem=w_recv.at[m, h, slot],
            device_id={"fs": fs_at(dj, di)}, device_id_type=MESH)
        cp.start()
        w_copies.append(cp)

    def w_wait(m, h, j, i):
        ref = piece(m, h, j, i)
        pltpu.make_async_copy(ref, ref, w_recv.at[m, h, j * X + i]).wait()

    def phase_one(ms):
        for m in ms:
            for i in range(1, X):
                w_copy(m, 0, 0, 0, 0, i)
            for j in range(1, Y):
                w_copy(m, 1, 0, 0, j, 0)

    def phase_own(ms):
        for m in ms:
            for i in range(1, X):
                w_copy(m, 1, 0, 0, 0, i)
            for j in range(1, Y):
                w_copy(m, 0, 0, 0, j, 0)

    def phase_relay(ms):
        for m in ms:
            for i in range(1, X):
                w_wait(m, 0, 0, i)
                for j in range(1, Y):
                    w_copy(m, 0, 0, i, j, 0)
            for j in range(1, Y):
                w_wait(m, 1, j, 0)
                for i in range(1, X):
                    w_copy(m, 1, j, 0, 0, i)

    def wait_cross(ms):
        for m in ms:
            for i in range(1, X):
                w_wait(m, 1, 0, i)
            for j in range(1, Y):
                w_wait(m, 0, j, 0)

    def wait_diag(ms):
        for m in ms:
            for j in range(1, Y):
                for i in range(1, X):
                    w_wait(m, 0, j, i)
                    w_wait(m, 1, j, i)

    def tok_chain(direction, s):
        src = z - s if direction == 0 else z + s
        dst = z + 1 if direction == 0 else z - 1
        ok = jnp.logical_and(src >= 0, dst < Z) if direction == 0 else jnp.logical_and(src < Z, dst >= 0)
        src, dst = jnp.clip(src, 0, Z - 1), jnp.clip(dst, 0, Z - 1)
        cp = pltpu.make_async_remote_copy(
            src_ref=nrm.at[c, src], dst_ref=nrm.at[c, src],
            send_sem=t_send.at[direction, s], recv_sem=t_recv.at[direction, s],
            device_id={"tp": tp_at(dst, c)}, device_id_type=MESH)
        return cp, ok

    def tok_sib(zz):
        return pltpu.make_async_remote_copy(
            src_ref=nrm.at[c, zz], dst_ref=nrm.at[c, zz],
            send_sem=ts_send.at[zz], recv_sem=ts_recv.at[zz],
            device_id={"tp": tp_at(z, sib)}, device_id_type=MESH)

    def tok_start(s):
        for direction in range(2):
            cp, ok = tok_chain(direction, s)
            pl.when(ok)(cp.start)

    def tok_arrive(s):
        for direction in range(2):
            src = z - s if direction == 0 else z + s
            there = src >= 0 if direction == 0 else src < Z
            src = jnp.clip(src, 0, Z - 1)

            @pl.when(there)
            def _():
                pltpu.make_async_copy(nrm.at[c, src], nrm.at[c, src], t_recv.at[direction, s - 1]).wait()
                if C > 1:
                    tok_sib(src).start()

            if s < Z - 1:
                cp, ok = tok_chain(direction, s)
                pl.when(ok)(cp.start)

    phase_one((0, 1))
    tok_start(0)
    if C > 1:
        tok_sib(z).start()
    phase_own((0, 1))
    if Z > 1:
        tok_arrive(1)
    phase_relay((0, 1))
    for s in range(2, Z):
        tok_arrive(s)
    wait_cross((0, 1))
    phase_one((2,))
    phase_own((2,))
    if C > 1:
        for zz in range(Z):
            ref = nrm.at[sib, zz]
            pltpu.make_async_copy(ref, ref, ts_recv.at[zz]).wait()

    near = [(0, 0)] + [(0, i) for i in range(1, X)] + [(j, 0) for j in range(1, Y)]
    far = [(j, i) for j in range(1, Y) for i in range(1, X)]
    mrows = tile * rows
    per_core = Z // tile

    def product(n, held, group):
        cc, zt = n // per_core, n % per_core
        total = None
        for j, i in group:
            o = fs_at(j, i)
            a = nrm[cc, pl.ds(zt * tile, tile), :, pl.ds(pl.multiple_of(o * K, K), K)].reshape(mrows, K)
            p = lax.dot_general(a, held[o], (((1,), (1,)), ((), ())), preferred_element_type=F32)
            total = p if total is None else total + p
        return total

    @pl.loop(0, C * per_core)
    def _(n):
        acc_g[n] = product(n, Wg, near)
        acc_u[n] = product(n, Wu, near)

    wait_diag((0,))

    @pl.loop(0, C * per_core)
    def _(n):
        g = acc_g[n]
        if far:
            g = g + product(n, Wg, far)
        acc_g[n] = jax.nn.silu(g)

    wait_diag((1,))

    @pl.loop(0, C * per_core)
    def _(n):
        u = acc_u[n]
        if far:
            u = u + product(n, Wu, far)
        hid[n // per_core, pl.ds((n % per_core) * tile, tile)] = (acc_g[n] * u).astype(BF16).reshape(tile, rows, H)

    sib_copies = []

    def sum_copy(q, direction, d):
        to = above if direction == 0 else below
        return pltpu.make_async_remote_copy(
            src_ref=rs_s.at[q, d], dst_ref=rs_r.at[q, direction, d],
            send_sem=q_send.at[q, d], recv_sem=q_recv.at[q, direction, d],
            device_id={"tp": tp_at(to, c)}, device_id_type=MESH)

    def sum_wait(q, direction, d):
        ref = rs_r.at[q, direction, d]
        pltpu.make_async_copy(ref, ref, q_recv.at[q, direction, d]).wait()

    units = []

    def down(new):
        qs = list(range(len(units), len(units) + len(new)))
        units.extend(new)

        def weight(q):
            j, i, h = units[q]
            return Wd[fs_at(j, i), :, h * N:(h + 1) * N]

        copies = []
        if C > 1:
            for q in qs:
                sib_s[q] = jnp.dot(hid[sib].reshape(Z * rows, H), weight(q),
                                   preferred_element_type=F32).astype(BF16).reshape(Z, rows, N)
                cp = pltpu.make_async_remote_copy(
                    src_ref=sib_s.at[q], dst_ref=sib_r.at[q], send_sem=p_send.at[q], recv_sem=p_recv.at[q],
                    device_id={"tp": tp_at(z, sib)}, device_id_type=MESH)
                cp.start()
                copies.append(cp)
        for q in qs:
            part[q] = jnp.dot(hid[c].reshape(Z * rows, H), weight(q),
                              preferred_element_type=F32).reshape(Z, rows, N)
        for q, cp in zip(qs, copies):
            cp.wait_recv()

            @pl.loop(0, Z)
            def _(d):
                part[q, d] = part[q, d] + sib_r[q, d].astype(F32)
        sib_copies.extend(copies)

        for direction, first, order in ((0, z == 0, range(Z - 1, 0, -1)), (1, z == Z - 1, range(Z - 1))):
            @pl.when(first)
            def _():
                for d in order:
                    for q in qs:
                        rs_s[q, d] = part[q, d].astype(BF16)
                        sum_copy(q, direction, d).start()
        return qs

    low = 2 * z < Z

    def sum_step(q, direction, d, ok):
        @pl.when(ok)
        def _():
            sum_wait(q, direction, d)
            rs_s[q, d] = (part[q, d] + rs_r[q, direction, d].astype(F32)).astype(BF16)
            sum_copy(q, direction, d).start()

    def sum_near(qs):
        for d in range(Z - 1, 0, -1):
            for q in qs:
                sum_step(q, 0, d, jnp.logical_and(jnp.logical_and(z > 0, z < d), low))
        for d in range(Z - 1):
            for q in qs:
                sum_step(q, 1, d, jnp.logical_and(jnp.logical_and(z < Z - 1, z > d), jnp.logical_not(low)))

    def sum_far(qs):
        for d in range(Z - 1, 0, -1):
            for q in qs:
                sum_step(q, 0, d, jnp.logical_and(z < d, jnp.logical_not(low)))
        for d in range(Z - 1):
            for q in qs:
                sum_step(q, 1, d, jnp.logical_and(z > d, low))

    def sum_end(q):
        j, i, h = units[q]
        for direction, there in ((0, z > 0), (1, z < Z - 1)):
            @pl.when(there)
            def _():
                sum_wait(q, direction, z)
                part[q, z] = part[q, z] + rs_r[q, direction, z].astype(F32)

        out[:, pl.ds(pl.multiple_of((fs_at(j, i) * cuts + h) * N, N), N)] = part[q, z].astype(BF16)

    in_row = [(0, i) for i in range(1, X)]
    in_col = [(j, 0) for j in range(1, Y)]
    both = range(cuts)
    early = [(j, i, 0) for j, i in in_row] + [(j, i, 1) for j, i in in_col] if cuts == 2 else []
    mid = [(j, i, h) for h in both for j, i in in_row + in_col if (j, i, h) not in early]
    qa = [q for h in both for q in down([(0, 0, h)])]
    phase_relay((2,))
    qb = down(early)
    sum_near(qa)
    wait_cross((2,))
    qc = down(mid)
    sum_near(qb)
    sum_far(qa)
    wait_diag((2,))
    qd = down([(j, i, h) for j, i in far for h in both])
    sum_near(qc)
    sum_far(qb)
    for q in qa + qb:
        sum_end(q)
    sum_far(qc)
    sum_near(qd)
    for q in qc:
        sum_end(q)
    sum_far(qd)
    for q in qd:
        sum_end(q)

    for cp in w_copies:
        cp.wait_send()
    for s in range(Z - 1):
        for direction in range(2):
            cp, ok = tok_chain(direction, s)
            pl.when(ok)(cp.wait_send)
    if C > 1:
        for zz in range(Z):
            tok_sib(zz).wait_send()
        for cp in sib_copies:
            cp.wait_send()
    for q in range(len(units)):
        for d in range(Z):
            pl.when(z != d)(sum_copy(q, 0, d).wait_send)


def local(sizes, tokens, norm_gain, gate_weight, up_weight, down_weight):
    Y, X, Z, C = sizes
    F = Y * X
    rows, D = tokens.shape
    gate_weight, up_weight = gate_weight.T, up_weight.T
    H, K = gate_weight.shape
    cuts = 2 if down_weight.shape[1] % 256 == 0 else 1
    N = down_weight.shape[1] // cuts
    U = F * cuts
    tile = 2 if Z % 2 == 0 else 1
    n_w = 3 * ((X - 1) + (Y - 1) * X + (Y - 1) + (X - 1) * Y)
    vmem = pl.BlockSpec(memory_space=pltpu.VMEM)
    dma = pltpu.SemaphoreType.DMA
    hbm = pl.BlockSpec(memory_space=pl.ANY)
    return pl.pallas_call(
        functools.partial(kernel, Y, X, Z, C, cuts),
        out_shape=pltpu.VMEM((rows, D), BF16),
        in_specs=[vmem] * 2 + [hbm] * 3,
        out_specs=vmem,
        scratch_shapes=[
            pltpu.VMEM((C, Z, rows, D), BF16),
            pltpu.VMEM((F, H, K), BF16),
            pltpu.VMEM((F, H, K), BF16),
            pltpu.VMEM((F, H, N * cuts), BF16),
            pltpu.VMEM((C * Z // tile, tile * rows, H), F32),
            pltpu.VMEM((C * Z // tile, tile * rows, H), F32),
            pltpu.VMEM((C, Z, rows, H), BF16),
            pltpu.VMEM((U, Z, rows, N), BF16),
            pltpu.VMEM((U, Z, rows, N), BF16),
            pltpu.VMEM((U, Z, rows, N), BF16),
            pltpu.VMEM((U, 2, Z, rows, N), BF16),
            pltpu.VMEM((U, Z, rows, N), F32),
            dma((3,)),
            dma((max(n_w, 1),)), dma((3, 2, F)),
            dma((2, Z)), dma((2, Z)), dma((Z,)), dma((Z,)),
            dma((U,)), dma((U,)), dma((U, Z)), dma((U, 2, Z)),
        ],
        compiler_params=pltpu.CompilerParams(
            collective_id=0, has_side_effects=True, vmem_limit_bytes=60 * 1024 * 1024),
    )(tokens, norm_gain.reshape(1, D), gate_weight, up_weight, down_weight)


def solution(mesh):
    fs, tp = mesh.shape["fs"], mesh.shape["tp"]
    X = max(n for n in range(1, math.isqrt(fs) + 1) if fs % n == 0)
    C = 2 if tp % 2 == 0 else 1
    from jax.sharding import PartitionSpec as P
    return jax.shard_map(
        functools.partial(local, (fs // X, X, tp // C, C)),
        mesh=mesh,
        in_specs=(P(("fs", "tp"), None), P(), P("fs", "tp"), P("fs", "tp"), P("tp", "fs")),
        out_specs=P(("fs", "tp"), None),
        check_vma=False,
    )
```

profile of v0, /device:TPU:4, one launch (start us, length us, event | category | flops | bytes accessed | tf_op | source)
XLA Modules:
  0.0 219.2 jit_solution(1882983371655780772)
XLA Ops:
  0.0 218.4 %shard_map.55 = bf16[128,2048]{1,0:T(8,128)(2,1)S(1)} custom-call(bf16[128,2048]{1,0:T(8,128)(2,1)} %tok.1, f32[1,2048]{1,0:T(1,128)} %bitcast.5, bf16[352,128]{1,0:T(8,128)(2,1)} %bitcast.3, bf16[352,128]{1,0:T(8,128)(2,1)} %bitcast.4, bf16[352,128]{1,0:T(8,128)(2,1)} %dw.1), custom_call_target="tpu_custom_call" | custom-call | tf_op jit(solution)/shard_map/pallas_call | solution.py:364
  218.4 0.8 copy.7
where the time goes:
time: 219 us
  Pallas kernels  218 us (100%)
    pallas_call x1, Pallas kernels, local(): pl.pallas_call(functools.partial(kernel, Y, X, Z, C, cuts), out_shape=plt...  218 us

commit v1 on v0

v1 whole, which is shorter than its diff:
```python
import jax
import jax.numpy as jnp
from jax import lax
from jax.experimental import pallas as pl
from jax.experimental.pallas import tpu as pltpu
from jax.sharding import PartitionSpec as P

eps_floor = 0.05
MESH = pl.DeviceIdType.MESH
F32 = jnp.float32
BF16 = jnp.bfloat16

SIDE, Z = 4, 8
ROWS, D, H = 128, 2048, 352
HALF = ROWS // 2
SLOTS = SIDE * SIDE
PAIRS = SLOTS // 2
UNITS = ((0, 0), (1, 0), (0, 1), (1, 1), (2, 0), (2, 1))
OWN, DOWN1, UP1, DOWN2, UP2 = 0, ROWS, 2 * ROWS, 3 * ROWS, 3 * ROWS + HALF
M = 4 * ROWS
SPAN = ((0, ROWS, -1), (ROWS, ROWS, 1), (2 * ROWS, HALF, -2), (2 * ROWS + HALF, HALF, 2))
WIDE = 2 * H
TILES = tuple((n, min(n + 256, WIDE)) for n in range(0, WIDE, 256))


def kernel(tok, gain, gw, uw, dw, out, T, W, G, hid, part, S, R,
           local, w_send, w_recv, s_send, s_recv, x_send, x_recv, t_send, t_recv, q_send, q_recv):
    f, t = lax.axis_index("fs"), lax.axis_index("tp")
    y, x, z, c = f // SIDE, f % SIDE, t // 2, t % 2

    def fs_at(j, i, core=c):
        dy = jnp.where(core == 0, j, i)
        dx = jnp.where(core == 0, i, j)
        return lax.rem(y + dy, SIDE) * SIDE + lax.rem(x + dx, SIDE)

    def z_at(dz):
        return {"tp": lax.rem(z + dz + Z, Z) * 2 + c}

    sib = {"tp": z * 2 + 1 - c}

    barrier = pltpu.get_barrier_semaphore()
    peers = [{"fs": fs_at(j, i)} for j, i in ((0, 1), (0, 3), (1, 0), (3, 0), (0, 2))]
    peers += [z_at(dz) for dz in (1, -1, 2, -2, 4)] + [sib]
    for peer in peers:
        pl.semaphore_signal(barrier, inc=1, device_id=peer, device_id_type=MESH)

    def piece(m, p, fs, core):
        return W.at[m, fs // 2, p, pl.ds(pl.multiple_of(core * H, 32), H),
                    pl.ds(pl.multiple_of((fs % 2) * 128, 128), 128)]

    own = [pltpu.make_async_copy(ref, piece(m, 0, f, c), local.at[m]) for m, ref in enumerate((gw, uw, dw))]
    for cp in own:
        cp.start()
    values = tok[...].astype(F32)
    factor = lax.rsqrt(jnp.mean(values * values, axis=-1, keepdims=True) + eps_floor)
    T[OWN:OWN + ROWS] = (values * factor * gain[...]).astype(BF16)
    pl.semaphore_wait(barrier, len(peers))
    for cp in own:
        cp.wait()

    sent = []

    def send(src, dst, send_sem, recv_sem, device):
        cp = pltpu.make_async_remote_copy(src_ref=src, dst_ref=dst, send_sem=send_sem, recv_sem=recv_sem,
                                          device_id=device, device_id_type=MESH)
        cp.start()
        sent.append(cp)

    def landed(ref, sem):
        pltpu.make_async_copy(ref, ref, sem).wait()

    count = [0]

    def hop(u, j, i, dj, di):
        m, p = UNITS[u]
        ref = piece(m, p, fs_at(j, i), c)
        slot = ((j - dj) % SIDE) * SIDE + (i - di) % SIDE
        send(ref, ref, w_send.at[count[0]], w_recv.at[u, slot], {"fs": fs_at(dj, di)})
        count[0] += 1

    def to_sib(u, j, i):
        m, p = UNITS[u]
        ref = piece(m, p, fs_at(j, i), c)
        k = j * SIDE + i
        send(ref, ref, s_send.at[u, k], s_recv.at[u, k], sib)

    def from_sib(u, j, i):
        m, p = UNITS[u]
        landed(piece(m, p, fs_at(j, i, 1 - c), 1 - c), s_recv.at[u, j * SIDE + i])

    def arrive(u, j, i):
        m, p = UNITS[u]
        landed(piece(m, p, fs_at(j, i), c), w_recv.at[u, j * SIDE + i])

    def exchange(m):
        send(piece(m, 0, f, c), piece(m, 1, f, c), x_send.at[m], x_recv.at[m], z_at(4))

    def begin(u):
        m, p = UNITS[u]
        if p == 1:
            landed(piece(m, 1, f, c), x_recv.at[m])
        for di in (1, 3, 2):
            hop(u, 0, 0, 0, di)
        for dj in (1, 3):
            hop(u, 0, 0, dj, 0)
        to_sib(u, 0, 0)

    def spread(u, i):
        arrive(u, 0, i)
        hop(u, 0, i, 1, 0)
        hop(u, 0, i, 3, 0)
        to_sib(u, 0, i)

    def relay(u, i):
        for j in ((3, 1) if i % 2 == 0 else (1, 3)):
            arrive(u, j, i)
            if i % 2 == 0 and j == 3:
                hop(u, 3, i, 1, 0)
            if i % 2 == 1 and j == 1:
                hop(u, 1, i, 3, 0)
            to_sib(u, j, i)

    def finish(u, i):
        arrive(u, 2, i)
        to_sib(u, 2, i)

    order = (0, 1, 3, 2)

    def tok_send(k, src, dst, dz):
        send(T.at[src:src + HALF], T.at[dst:dst + HALF], t_send.at[k], t_recv.at[k], z_at(dz))

    def tok_wait(k, dst):
        landed(T.at[dst:dst + HALF], t_recv.at[k])

    def all_sib(u):
        for j in range(SIDE):
            for i in range(SIDE):
                from_sib(u, j, i)

    def wide_dot(m, p, n0, n1):
        total = None
        for q in range(PAIRS):
            d = lax.dot_general(T[:, q * 256:(q + 1) * 256], W[m, q, p, n0:n1, :],
                                (((1,), (1,)), ((), ())), preferred_element_type=F32)
            total = d if total is None else total + d
        return total

    def gate(p):
        for n0, n1 in TILES:
            G[:, n0:n1] = wide_dot(0, p, n0, n1)

    def up(p):
        for n0, n1 in TILES:
            hid[p, :, n0:n1] = (jax.nn.silu(G[:, n0:n1]) * wide_dot(1, p, n0, n1)).astype(BF16)

    def pair_of(oy, px):
        return lax.rem(y + oy, SIDE) * 2 + px

    def down(oy):
        @pl.loop(0, 2)
        def _(px):
            q = pair_of(oy, px)
            total = None
            for p in range(2):
                d = jnp.dot(hid[p], W[2, q, p], preferred_element_type=F32)
                total = d if total is None else total + d
            part[q] = total[:ROWS]
            S[q] = total[ROWS:].astype(BF16)
            for k, (r0, n, dz) in enumerate(SPAN):
                pltpu.make_async_remote_copy(
                    src_ref=S.at[q, r0:r0 + n], dst_ref=R.at[q, r0:r0 + n],
                    send_sem=q_send.at[oy, px, k], recv_sem=q_recv.at[oy, px, k],
                    device_id=z_at(dz), device_id_type=MESH).start()

    def total_of(oy):
        @pl.loop(0, 2)
        def _(px):
            q = pair_of(oy, px)
            for k, (r0, n, dz) in enumerate(SPAN):
                landed(R.at[q, r0:r0 + n], q_recv.at[oy, px, k])
            for h in range(2):
                a = h * HALF
                total = part[q, a:a + HALF] + R[q, a:a + HALF].astype(F32)
                total = total + R[q, ROWS + a:ROWS + a + HALF].astype(F32)
                total = total + R[q, 2 * ROWS + a:2 * ROWS + a + HALF].astype(F32)
                out[a:a + HALF, pl.ds(pl.multiple_of(q * 256, 256), 256)] = total.astype(BF16)

    begin(0)
    exchange(0)
    tok_send(0, OWN, DOWN1, 1)
    tok_send(1, OWN + HALF, UP1 + HALF, -1)
    exchange(1)
    tok_send(2, OWN + HALF, DOWN1 + HALF, 1)
    tok_send(3, OWN, UP1, -1)
    begin(1)
    for i in (1, 3, 2):
        spread(0, i)
    begin(2)
    for i in (1, 3, 2):
        spread(1, i)
    for i in order:
        relay(0, i)
    tok_wait(0, DOWN1)
    tok_send(4, DOWN1, DOWN2, 1)
    tok_wait(1, UP1 + HALF)
    tok_send(5, UP1 + HALF, UP2, -1)
    exchange(2)
    begin(3)
    for i in (1, 3, 2):
        spread(2, i)
    for i in order:
        relay(1, i)
    for i in order:
        finish(0, i)
    begin(4)
    for i in (1, 3, 2):
        spread(3, i)
    for i in order:
        relay(2, i)
    for i in order:
        finish(1, i)
    begin(5)
    tok_wait(2, DOWN1 + HALF)
    tok_wait(3, UP1)
    tok_wait(4, DOWN2)
    tok_wait(5, UP2)
    all_sib(0)
    gate(0)
    for i in (1, 3, 2):
        spread(4, i)
        spread(5, i)
    for i in order:
        relay(3, i)
    all_sib(1)
    up(0)
    for i in order:
        finish(2, i)
    for u in (4, 5):
        relay(u, 0)
    all_sib(2)
    gate(1)
    for i in order:
        finish(3, i)
    for u in (4, 5):
        relay(u, 1)
    all_sib(3)
    up(1)
    for u in (4, 5):
        finish(u, 0)
    for u in (4, 5):
        for j, i in [(0, n) for n in range(SIDE)] + [(n, 0) for n in range(1, SIDE)]:
            from_sib(u, j, i)
    down(0)
    for i in (3, 2):
        for u in (4, 5):
            relay(u, i)
    for u in (4, 5):
        finish(u, 1)
    for u in (4, 5):
        for j, i in ((1, 1), (1, 2), (1, 3), (2, 1), (3, 1)):
            from_sib(u, j, i)
    down(1)
    for u in (4, 5):
        finish(u, 3)
    for u in (4, 5):
        for j, i in ((3, 3), (2, 3), (3, 2)):
            from_sib(u, j, i)
    down(3)
    for u in (4, 5):
        finish(u, 2)
    for u in (4, 5):
        from_sib(u, 2, 2)
    down(2)
    for oy in order:
        total_of(oy)

    for cp in sent:
        cp.wait_send()

    @pl.loop(0, PAIRS)
    def _(n):
        oy, px = n // 2, n % 2
        for k, (r0, rows, dz) in enumerate(SPAN):
            ref = S.at[pair_of(oy, px), r0:r0 + rows]
            pltpu.make_async_copy(ref, ref, q_send.at[oy, px, k]).wait()


def layer(tokens, norm_gain, gate_weight, up_weight, down_weight):
    vmem = pl.BlockSpec(memory_space=pltpu.VMEM)
    hbm = pl.BlockSpec(memory_space=pl.ANY)
    dma = pltpu.SemaphoreType.DMA
    n_hops = len(UNITS) * (SLOTS - 1)
    return pl.pallas_call(
        kernel,
        out_shape=pltpu.VMEM((ROWS, D), BF16),
        in_specs=[vmem] * 2 + [hbm] * 3,
        out_specs=vmem,
        scratch_shapes=[
            pltpu.VMEM((M, D), BF16),
            pltpu.VMEM((3, PAIRS, 2, WIDE, 256), BF16),
            pltpu.VMEM((M, WIDE), F32),
            pltpu.VMEM((2, M, WIDE), BF16),
            pltpu.VMEM((PAIRS, ROWS, 256), F32),
            pltpu.VMEM((PAIRS, M - ROWS, 256), BF16),
            pltpu.VMEM((PAIRS, M - ROWS, 256), BF16),
            dma((3,)),
            dma((n_hops,)), dma((len(UNITS), SLOTS)),
            dma((len(UNITS), SLOTS)), dma((len(UNITS), SLOTS)),
            dma((3,)), dma((3,)),
            dma((6,)), dma((6,)),
            dma((SIDE, 2, 4)), dma((SIDE, 2, 4)),
        ],
        compiler_params=pltpu.CompilerParams(
            collective_id=0, has_side_effects=True, vmem_limit_bytes=60 * 1024 * 1024),
    )(tokens, norm_gain.reshape(1, D), gate_weight.T, up_weight.T, down_weight)


def solution(mesh):
    return jax.shard_map(
        layer,
        mesh=mesh,
        in_specs=(P(("fs", "tp"), None), P(), P("fs", "tp"), P("fs", "tp"), P("tp", "fs")),
        out_specs=P(("fs", "tp"), None),
        check_vma=False,
    )
```

time: 219 us -> 91.7 us (0.42)
  Pallas kernels: 218 us -> 89.7 us
    pallas_call x1, Pallas kernels: 218 us -> 89.7 us  [layer(): pl.pallas_call(kernel, out_shape=pltpu.VMEM((ROWS, D), BF16), in_specs=[v...]
where the time goes in v1:
time: 91.7 us; the launch traced here: 90.5 us
  Pallas kernels  89.7 us (98%)
    pallas_call x1, Pallas kernels, layer(): pl.pallas_call(kernel, out_shape=pltpu.VMEM((ROWS, D), BF16), in_specs=[v...  89.7 us

profile of v1, /device:TPU:4, one launch (start us, length us, event | category | flops | bytes accessed | tf_op | source)
XLA Modules:
  0.0 90.5 jit_solution(1988833405839446507)
XLA Ops:
  0.0 89.7 %shard_map.55 = bf16[128,2048]{1,0:T(8,128)(2,1)S(1)} custom-call(bf16[128,2048]{1,0:T(8,128)(2,1)} %tok.1, f32[1,2048]{1,0:T(1,128)} %bitcast.5, bf16[352,128]{1,0:T(8,128)(2,1)} %bitcast.3, bf16[352,128]{1,0:T(8,128)(2,1)} %bitcast.4, bf16[352,128]{1,0:T(8,128)(2,1)} %dw.1), custom_call_target="tpu_custom_call" | custom-call | tf_op jit(solution)/shard_map/pallas_call | solution.py:293
  89.7 0.8 copy.7

commit v2 on v1

v2 whole, which is shorter than its diff:
```python
import jax
import jax.numpy as jnp
from jax import lax
from jax.experimental import pallas as pl
from jax.experimental.pallas import tpu as pltpu
from jax.sharding import PartitionSpec as P

eps_floor = 0.05
MESH = pl.DeviceIdType.MESH
F32 = jnp.float32
BF16 = jnp.bfloat16

SIDE, Z = 4, 8
ROWS, D, H = 128, 2048, 352
HALF = ROWS // 2
SLOTS = SIDE * SIDE
PAIRS = SLOTS // 2
UNITS = ((0, 0), (1, 0), (0, 1), (1, 1), (2, 0), (2, 1))
OWN, DOWN1, UP1, DOWN2, UP2 = 0, ROWS, 2 * ROWS, 3 * ROWS, 3 * ROWS + HALF
M = 4 * ROWS
FIRST = ((0, -1, DOWN2), (1, -1, DOWN1 + HALF), (3, 1, UP2), (4, 1, UP1))
SECOND = ((2, -1, 0, ROWS), (5, 1, 3, ROWS + HALF))
WIDE = 2 * H
STEPS = ((0, 0), (0, 1), (1, 0), (3, 0), (2, 0), (1, 1), (3, 1), (2, 1))
NEEDS = {0: ((0, 0), (0, 1), (0, 3), (1, 0), (3, 0)), 1: ((0, 2), (2, 0)), 2: ((1, 1), (1, 3), (3, 1)), 3: ((3, 3),),
         4: ((2, 1), (2, 3), (1, 2), (3, 2)), 7: ((2, 2),)}
SET_OF = {piece: step for step, pieces in NEEDS.items() for piece in pieces}
TILES = tuple((n, min(n + 256, WIDE)) for n in range(0, WIDE, 256))


def kernel(tok, gain, gw, uw, dw, out, raw, T, W, G, hid, part, S, R,
           local, w_send, w_recv, s_send, s_recv, x_send, x_recv, t_send, t_recv, q_send, q_recv):
    f, t = lax.axis_index("fs"), lax.axis_index("tp")
    y, x, z, c = f // SIDE, f % SIDE, t // 2, t % 2

    def fs_at(j, i, core=c):
        dy = jnp.where(core == 0, j, i)
        dx = jnp.where(core == 0, i, j)
        return lax.rem(y + dy, SIDE) * SIDE + lax.rem(x + dx, SIDE)

    def z_at(dz):
        return {"tp": lax.rem(z + dz + Z, Z) * 2 + c}

    sib = {"tp": z * 2 + 1 - c}

    barrier = pltpu.get_barrier_semaphore()
    peers = [{"fs": fs_at(j, i)} for j, i in ((0, 1), (0, 3), (1, 0), (3, 0), (0, 2))]
    peers += [z_at(dz) for dz in (1, -1, 4)] + [sib]
    for peer in peers:
        pl.semaphore_signal(barrier, inc=1, device_id=peer, device_id_type=MESH)

    def piece(m, p, fs, core):
        return W.at[m, fs // 2, p, pl.ds(pl.multiple_of(core * H, 32), H),
                    pl.ds(pl.multiple_of((fs % 2) * 128, 128), 128)]

    own = [pltpu.make_async_copy(ref, piece(m, 0, f, c), local.at[m]) for m, ref in enumerate((gw, uw, dw))]
    raw_copy = pltpu.make_async_copy(tok, raw, local.at[3])
    for cp in own:
        cp.start()
    raw_copy.start()
    pl.semaphore_wait(barrier, len(peers))
    for cp in own:
        cp.wait()

    def send(src, dst, send_sem, recv_sem, device):
        cp = pltpu.make_async_remote_copy(src_ref=src, dst_ref=dst, send_sem=send_sem, recv_sem=recv_sem,
                                          device_id=device, device_id_type=MESH)
        cp.start()

    def landed(ref, sem):
        pltpu.make_async_copy(ref, ref, sem).wait()

    def hop(u, j, i, dj, di):
        m, p = UNITS[u]
        ref = piece(m, p, fs_at(j, i), c)
        slot = ((j - dj) % SIDE) * SIDE + (i - di) % SIDE
        send(ref, ref, w_send.at[u], w_recv.at[u, slot], {"fs": fs_at(dj, di)})

    def to_sib(u, j, i):
        m, p = UNITS[u]
        ref = piece(m, p, fs_at(j, i), c)
        k = u if u < 4 else 4 + SET_OF[j, i]
        send(ref, ref, s_send.at[u], s_recv.at[k], sib)

    def half_of(core):
        return pl.ds(pl.multiple_of(core * H, 32), H)

    def all_sib(u):
        m, p = UNITS[u]
        landed(W.at[m, :, p, half_of(1 - c), :], s_recv.at[u])

    def set_sib(step):
        landed(W.at[2, 0:len(NEEDS[step]), :, half_of(1 - c), 0:128], s_recv.at[4 + step])

    def arrive(u, j, i):
        m, p = UNITS[u]
        landed(piece(m, p, fs_at(j, i), c), w_recv.at[u, j * SIDE + i])

    def exchange(m):
        send(piece(m, 0, f, c), piece(m, 1, f, c), x_send, x_recv.at[m], z_at(4))

    def begin(u):
        m, p = UNITS[u]
        if p == 1:
            landed(piece(m, 1, f, c), x_recv.at[m])
        for di in (1, 3, 2):
            hop(u, 0, 0, 0, di)
        for dj in (1, 3):
            hop(u, 0, 0, dj, 0)
        to_sib(u, 0, 0)

    def spread(u, i):
        arrive(u, 0, i)
        hop(u, 0, i, 1, 0)
        hop(u, 0, i, 3, 0)
        to_sib(u, 0, i)

    def relay(u, i):
        for j in ((3, 1) if i % 2 == 0 else (1, 3)):
            arrive(u, j, i)
            if i % 2 == 0 and j == 3:
                hop(u, 3, i, 1, 0)
            if i % 2 == 1 and j == 1:
                hop(u, 1, i, 3, 0)
            to_sib(u, j, i)

    def finish(u, i):
        arrive(u, 2, i)
        to_sib(u, 2, i)

    order = (0, 1, 3, 2)

    def tok_send(k, src, dst, dz):
        send(T.at[src:src + HALF], T.at[dst:dst + HALF], t_send, t_recv.at[k], z_at(dz))

    def tok_wait(k, dst):
        landed(T.at[dst:dst + HALF], t_recv.at[k])

    def wide_dot(m, p, n0, n1):
        total = None
        for q in range(PAIRS):
            d = lax.dot_general(T[:, q * 256:(q + 1) * 256], W[m, q, p, n0:n1, :],
                                (((1,), (1,)), ((), ())), preferred_element_type=F32)
            total = d if total is None else total + d
        return total

    def gate(p):
        for n0, n1 in TILES:
            G[:, n0:n1] = wide_dot(0, p, n0, n1)

    def up(p):
        for n0, n1 in TILES:
            hid[p, :, n0:n1] = (jax.nn.silu(G[:, n0:n1]) * wide_dot(1, p, n0, n1)).astype(BF16)

    def pair_of(step):
        dy, far = STEPS[step]
        px = x // 2
        return lax.rem(y + dy, SIDE) * 2 + (1 - px if far else px)

    def sum_send(step, k, dz):
        q = pair_of(step)
        lot = (0, 2, 2, 1, 2, 2)[k]
        send(S.at[q, k], R.at[q, k], q_send, q_recv.at[step, lot], z_at(dz))

    def down(step):
        q = pair_of(step)
        total = None
        for p in range(2):
            d = jnp.dot(hid[p], W[2, q, p], preferred_element_type=F32)
            total = d if total is None else total + d
        part[q, :ROWS] = total[:ROWS]
        part[q, ROWS:ROWS + HALF] = total[DOWN1:DOWN1 + HALF]
        part[q, ROWS + HALF:] = total[UP1 + HALF:UP1 + ROWS]
        for k, dz, r0 in FIRST:
            S[q, k] = total[r0:r0 + HALF].astype(BF16)
            sum_send(step, k, dz)

    def pass_on(step):
        q = pair_of(step)
        for lot, (k, dz, source, r0) in enumerate(SECOND):
            landed(R.at[q, source], q_recv.at[step, lot])
            S[q, k] = (part[q, r0:r0 + HALF] + R[q, source].astype(F32)).astype(BF16)
            sum_send(step, k, dz)

    def total_of(step):
        q = pair_of(step)
        landed(R.at[q, 0:4], q_recv.at[step, 2])
        for a, first, second in ((0, 4, 2), (HALF, 1, 5)):
            total = part[q, a:a + HALF] + R[q, first].astype(F32) + R[q, second].astype(F32)
            out[a:a + HALF, pl.ds(pl.multiple_of(q * 256, 256), 256)] = total.astype(BF16)

    begin(0)
    exchange(0)
    begin(1)
    exchange(1)
    raw_copy.wait()
    values = raw[...].astype(F32)
    factor = lax.rsqrt(jnp.mean(values * values, axis=-1, keepdims=True) + eps_floor)
    T[OWN:OWN + ROWS] = (values * factor * gain[...]).astype(BF16)
    for i in (1, 3, 2):
        spread(0, i)
    tok_send(0, OWN, DOWN1, 1)
    tok_send(1, OWN + HALF, UP1 + HALF, -1)
    tok_send(2, OWN + HALF, DOWN1 + HALF, 1)
    tok_send(3, OWN, UP1, -1)
    begin(2)
    for i in (1, 3, 2):
        spread(1, i)
    for i in order:
        relay(0, i)
    tok_wait(0, DOWN1)
    tok_send(4, DOWN1, DOWN2, 1)
    tok_wait(1, UP1 + HALF)
    tok_send(5, UP1 + HALF, UP2, -1)
    exchange(2)
    begin(3)
    for i in (1, 3, 2):
        spread(2, i)
    for i in order:
        relay(1, i)
    for i in order:
        finish(0, i)
    for i in (1, 3, 2):
        spread(3, i)
    begin(4)
    for i in order:
        relay(2, i)
    for i in order:
        finish(1, i)
    tok_wait(2, DOWN1 + HALF)
    tok_wait(3, UP1)
    tok_wait(4, DOWN2)
    tok_wait(5, UP2)
    all_sib(0)
    gate(0)
    begin(5)
    for i in order:
        relay(3, i)
    all_sib(1)
    up(0)
    for i in order:
        finish(2, i)
    for u in (4, 5):
        relay(u, 0)
    all_sib(2)
    gate(1)
    for i in (1, 3, 2):
        spread(4, i)
        spread(5, i)
    for i in order:
        finish(3, i)
    all_sib(3)
    up(1)
    set_sib(0)
    down(0)
    for u in (4, 5):
        finish(u, 0)
    for i in (1, 3):
        for u in (4, 5):
            relay(u, i)
    set_sib(1)
    down(1)
    pass_on(0)
    set_sib(2)
    down(2)
    pass_on(1)
    for u in (4, 5):
        relay(u, 2)
    set_sib(3)
    down(3)
    pass_on(2)
    for i in (1, 3):
        for u in (4, 5):
            finish(u, i)
    pass_on(3)
    set_sib(4)
    down(4)
    down(5)
    pass_on(4)
    down(6)
    for u in (4, 5):
        finish(u, 2)
    pass_on(5)
    pass_on(6)
    set_sib(7)
    down(7)
    for step in range(6):
        total_of(step)
    pass_on(7)
    total_of(6)
    total_of(7)

    for u, (m, p) in enumerate(UNITS):
        landed(W.at[:, 0:5, 0, 0:H, 0:128], w_send.at[u])
        landed(W.at[m, :, p, half_of(c), :], s_send.at[u])
    landed(W.at[:, 0, 0, 0:H, 0:128], x_send)
    landed(T.at[0:6 * HALF], t_send)
    landed(S, q_send)


def layer(tokens, norm_gain, gate_weight, up_weight, down_weight):
    vmem = pl.BlockSpec(memory_space=pltpu.VMEM)
    hbm = pl.BlockSpec(memory_space=pl.ANY)
    dma = pltpu.SemaphoreType.DMA
    return pl.pallas_call(
        kernel,
        out_shape=pltpu.VMEM((ROWS, D), BF16),
        in_specs=[hbm, vmem] + [hbm] * 3,
        out_specs=vmem,
        scratch_shapes=[
            pltpu.VMEM((ROWS, D), BF16),
            pltpu.VMEM((M, D), BF16),
            pltpu.VMEM((3, PAIRS, 2, WIDE, 256), BF16),
            pltpu.VMEM((M, WIDE), F32),
            pltpu.VMEM((2, M, WIDE), BF16),
            pltpu.VMEM((PAIRS, 2 * ROWS, 256), F32),
            pltpu.VMEM((PAIRS, 6, HALF, 256), BF16),
            pltpu.VMEM((PAIRS, 6, HALF, 256), BF16),
            dma((4,)),
            dma((len(UNITS),)), dma((len(UNITS), SLOTS)),
            dma((len(UNITS),)), dma((4 + len(STEPS),)),
            dma, dma((3,)),
            dma, dma((6,)),
            dma, dma((len(STEPS), 3)),
        ],
        compiler_params=pltpu.CompilerParams(
            collective_id=0, has_side_effects=True, vmem_limit_bytes=60 * 1024 * 1024),
    )(tokens, norm_gain.reshape(1, D), gate_weight.T, up_weight.T, down_weight)


def solution(mesh):
    return jax.shard_map(
        layer,
        mesh=mesh,
        in_specs=(P(("fs", "tp"), None), P(), P("fs", "tp"), P("fs", "tp"), P("tp", "fs")),
        out_specs=P(("fs", "tp"), None),
        check_vma=False,
    )
```

time: 91.7 us -> 84.7 us (0.924)
  Pallas kernels: 89.7 us -> 83.4 us
    pallas_call x1, Pallas kernels: 89.7 us -> 83.4 us  [layer(): pl.pallas_call(kernel, out_shape=pltpu.VMEM((ROWS, D), BF16), in_specs=[h...]
where the time goes in v2:
time: 84.7 us; the launch traced here: 84.2 us
  Pallas kernels  83.4 us (98%)
    pallas_call x1, Pallas kernels, layer(): pl.pallas_call(kernel, out_shape=pltpu.VMEM((ROWS, D), BF16), in_specs=[h...  83.4 us

profile of v2, /device:TPU:4, one launch (start us, length us, event | category | flops | bytes accessed | tf_op | source)
XLA Modules:
  0.0 84.2 jit_solution(5638737866197187176)
XLA Ops:
  0.0 83.4 %shard_map.55 = bf16[128,2048]{1,0:T(8,128)(2,1)S(1)} custom-call(bf16[128,2048]{1,0:T(8,128)(2,1)} %tok.1, f32[1,2048]{1,0:T(1,128)} %bitcast.5, bf16[352,128]{1,0:T(8,128)(2,1)} %bitcast.3, bf16[352,128]{1,0:T(8,128)(2,1)} %bitcast.4, bf16[352,128]{1,0:T(8,128)(2,1)} %dw.1), custom_call_target="tpu_custom_call" | custom-call | tf_op jit(solution)/shard_map/pallas_call | solution.py:305
  83.4 0.8 copy.7

commit v3 on v2

--- a/solution.py
+++ b/solution.py
@@ -197,32 +197,31 @@
     values = raw[...].astype(F32)
     factor = lax.rsqrt(jnp.mean(values * values, axis=-1, keepdims=True) + eps_floor)
     T[OWN:OWN + ROWS] = (values * factor * gain[...]).astype(BF16)
-    for i in (1, 3, 2):
-        spread(0, i)
     tok_send(0, OWN, DOWN1, 1)
     tok_send(1, OWN + HALF, UP1 + HALF, -1)
     tok_send(2, OWN + HALF, DOWN1 + HALF, 1)
     tok_send(3, OWN, UP1, -1)
+    for i in (1, 3, 2):
+        spread(0, i)
     begin(2)
     for i in (1, 3, 2):
         spread(1, i)
     for i in order:
         relay(0, i)
+    begin(3)
+    for i in (1, 3, 2):
+        spread(2, i)
     tok_wait(0, DOWN1)
     tok_send(4, DOWN1, DOWN2, 1)
     tok_wait(1, UP1 + HALF)
     tok_send(5, UP1 + HALF, UP2, -1)
     exchange(2)
-    begin(3)
-    for i in (1, 3, 2):
-        spread(2, i)
     for i in order:
         relay(1, i)
     for i in order:
         finish(0, i)
     for i in (1, 3, 2):
         spread(3, i)
-    begin(4)
     for i in order:
         relay(2, i)
     for i in order:
@@ -233,62 +232,64 @@
     tok_wait(5, UP2)
     all_sib(0)
     gate(0)
+    for i in order:
+        relay(3, i)
+    begin(4)
     begin(5)
-    for i in order:
-        relay(3, i)
     all_sib(1)
     up(0)
     for i in order:
         finish(2, i)
     for u in (4, 5):
-        relay(u, 0)
+        for i in (1, 3):
+            spread(u, i)
     all_sib(2)
     gate(1)
-    for i in (1, 3, 2):
-        spread(4, i)
-        spread(5, i)
     for i in order:
         finish(3, i)
+    for u in (4, 5):
+        relay(u, 0)
+        spread(u, 2)
     all_sib(3)
     up(1)
     set_sib(0)
     down(0)
     for u in (4, 5):
         finish(u, 0)
-    for i in (1, 3):
-        for u in (4, 5):
-            relay(u, i)
+    for u in (4, 5):
+        relay(u, 1)
     set_sib(1)
     down(1)
-    pass_on(0)
+    for u in (4, 5):
+        relay(u, 3)
     set_sib(2)
     down(2)
-    pass_on(1)
-    for u in (4, 5):
-        relay(u, 2)
+    pass_on(0)
     set_sib(3)
     down(3)
-    pass_on(2)
+    for u in (4, 5):
+        relay(u, 2)
+    pass_on(1)
     for i in (1, 3):
         for u in (4, 5):
             finish(u, i)
-    pass_on(3)
+    pass_on(2)
     set_sib(4)
     down(4)
+    pass_on(3)
     down(5)
-    pass_on(4)
     down(6)
     for u in (4, 5):
         finish(u, 2)
-    pass_on(5)
-    pass_on(6)
     set_sib(7)
     down(7)
-    for step in range(6):
+    for step in (4, 5, 6):
+        pass_on(step)
+    for step in range(4):
         total_of(step)
     pass_on(7)
-    total_of(6)
-    total_of(7)
+    for step in range(4, len(STEPS)):
+        total_of(step)
 
     for u, (m, p) in enumerate(UNITS):
         landed(W.at[:, 0:5, 0, 0:H, 0:128], w_send.at[u])

time: 84.7 us -> 80.5 us (0.950)
  the two profiles are of different devices: /device:TPU:4 before, /device:TPU:1 now
where the time goes in v3:
time: 80.5 us; the launch traced here: 80.4 us
  Pallas kernels  79.6 us (99%)
    pallas_call x1, Pallas kernels, layer(): pl.pallas_call(kernel, out_shape=pltpu.VMEM((ROWS, D), BF16), in_specs=[h...  79.6 us

profile of v3, /device:TPU:1, one launch (start us, length us, event | category | flops | bytes accessed | tf_op | source)
XLA Modules:
  0.0 80.4 jit_solution(10414535485084369343)
XLA Ops:
  0.0 79.6 %shard_map.55 = bf16[128,2048]{1,0:T(8,128)(2,1)S(1)} custom-call(bf16[128,2048]{1,0:T(8,128)(2,1)} %tok.1, f32[1,2048]{1,0:T(1,128)} %bitcast.5, bf16[352,128]{1,0:T(8,128)(2,1)} %bitcast.3, bf16[352,128]{1,0:T(8,128)(2,1)} %bitcast.4, bf16[352,128]{1,0:T(8,128)(2,1)} %dw.1), custom_call_target="tpu_custom_call" | custom-call | tf_op jit(solution)/shard_map/pallas_call | solution.py:306
  79.6 0.8 copy.7

commit v4 on v3

--- a/solution.py
+++ b/solution.py
@@ -226,16 +226,16 @@
         relay(2, i)
     for i in order:
         finish(1, i)
+    for i in order:
+        relay(3, i)
+    begin(4)
+    begin(5)
     tok_wait(2, DOWN1 + HALF)
     tok_wait(3, UP1)
     tok_wait(4, DOWN2)
     tok_wait(5, UP2)
     all_sib(0)
     gate(0)
-    for i in order:
-        relay(3, i)
-    begin(4)
-    begin(5)
     all_sib(1)
     up(0)
     for i in order:
@@ -251,24 +251,24 @@
         relay(u, 0)
         spread(u, 2)
     all_sib(3)
+    for u in (4, 5):
+        relay(u, 1)
     up(1)
     set_sib(0)
     down(0)
     for u in (4, 5):
+        relay(u, 3)
+    for u in (4, 5):
         finish(u, 0)
-    for u in (4, 5):
-        relay(u, 1)
     set_sib(1)
     down(1)
     for u in (4, 5):
-        relay(u, 3)
+        relay(u, 2)
     set_sib(2)
     down(2)
     pass_on(0)
     set_sib(3)
     down(3)
-    for u in (4, 5):
-        relay(u, 2)
     pass_on(1)
     for i in (1, 3):
         for u in (4, 5):

time: 80.5 us -> 78.9 us (0.980)
  the two profiles are of different devices: /device:TPU:1 before, /device:TPU:4 now
where the time goes in v4:
time: 78.9 us; the launch traced here: 77.5 us
  Pallas kernels  76.7 us (97%)
  local copies, waits for them, and re-layouts  0.8 us (1%)
    pallas_call x1, Pallas kernels, layer(): pl.pallas_call(kernel, out_shape=pltpu.VMEM((ROWS, D), BF16), in_specs=[h...  76.7 us

profile of v4, /device:TPU:4, one launch (start us, length us, event | category | flops | bytes accessed | tf_op | source)
XLA Modules:
  0.0 77.5 jit_solution(8985531370063985228)
XLA Ops:
  0.0 76.7 %shard_map.55 = bf16[128,2048]{1,0:T(8,128)(2,1)S(1)} custom-call(bf16[128,2048]{1,0:T(8,128)(2,1)} %tok.1, f32[1,2048]{1,0:T(1,128)} %bitcast.5, bf16[352,128]{1,0:T(8,128)(2,1)} %bitcast.3, bf16[352,128]{1,0:T(8,128)(2,1)} %bitcast.4, bf16[352,128]{1,0:T(8,128)(2,1)} %dw.1), custom_call_target="tpu_custom_call" | custom-call | tf_op jit(solution)/shard_map/pallas_call | solution.py:306
  76.7 0.8 %copy.7 = bf16[128,2048]{1,0:T(8,128)(2,1)} copy(bf16[128,2048]{1,0:T(8,128)(2,1)S(1)} %shard_map.55) | data formatting | bytes 1048576

commit v5 on v4

--- a/solution.py
+++ b/solution.py
@@ -236,13 +236,13 @@
     tok_wait(5, UP2)
     all_sib(0)
     gate(0)
+    for u in (4, 5):
+        for i in (1, 3):
+            spread(u, i)
     all_sib(1)
     up(0)
     for i in order:
         finish(2, i)
-    for u in (4, 5):
-        for i in (1, 3):
-            spread(u, i)
     all_sib(2)
     gate(1)
     for i in order:

time: 78.9 us -> 82.1 us (1.041)
  Pallas kernels: 76.7 us -> 80.2 us
    pallas_call x1, Pallas kernels: 76.7 us -> 80.2 us  [layer(): pl.pallas_call(kernel, out_shape=pltpu.VMEM((ROWS, D), BF16), in_specs=[h...]
where the time goes in v5:
time: 82.1 us; the launch traced here: 81 us
  Pallas kernels  80.2 us (98%)
    pallas_call x1, Pallas kernels, layer(): pl.pallas_call(kernel, out_shape=pltpu.VMEM((ROWS, D), BF16), in_specs=[h...  80.2 us

profile of v5, /device:TPU:4, one launch (start us, length us, event | category | flops | bytes accessed | tf_op | source)
XLA Modules:
  0.0 81.0 jit_solution(10782368160715049254)
XLA Ops:
  0.0 80.2 %shard_map.55 = bf16[128,2048]{1,0:T(8,128)(2,1)S(1)} custom-call(bf16[128,2048]{1,0:T(8,128)(2,1)} %tok.1, f32[1,2048]{1,0:T(1,128)} %bitcast.5, bf16[352,128]{1,0:T(8,128)(2,1)} %bitcast.3, bf16[352,128]{1,0:T(8,128)(2,1)} %bitcast.4, bf16[352,128]{1,0:T(8,128)(2,1)} %dw.1), custom_call_target="tpu_custom_call" | custom-call | tf_op jit(solution)/shard_map/pallas_call | solution.py:306
  80.2 0.8 copy.7
